TPU v7x, 32 devices: a whole 2x2x4 slice. The times are simulated.
32 devices in a mesh: sp: 8 (over z, y), tp: 4 (over x, core).
Axes of the slice: x: 2, y: 2, z: 4, core: 2. Of those that a mesh axis runs over, the one named last changes fastest.
Arguments:
- tokens: bfloat16 [1024, 2048], P(('sp', 'tp')), may hold values from -6 to 6
- doc_lengths: int32 [16], replicated, may hold values from 1 to 640, 1024 in all
- query_down: bfloat16 [2048, 512], replicated, may hold values from -0.125 to 0.125
- latent_down: bfloat16 [2048, 256], replicated, may hold values from -0.125 to 0.125
- rope_down: bfloat16 [2048, 32], replicated, may hold values from -0.125 to 0.125
- query_latent_gain: float32 [512], replicated, may hold values from 0.1 to 1.9
- latent_gain: float32 [256], replicated, may hold values from 0.1 to 1.9
- query_up: bfloat16 [512, 768], P(None, 'tp'), may hold values from -0.25 to 0.25
- key_up: bfloat16 [256, 512], P(None, 'tp'), may hold values from -0.375 to 0.375
- value_up: bfloat16 [256, 512], P(None, 'tp'), may hold values from -0.375 to 0.375
- query_gain: float32 [96], replicated, may hold values from 0.5 to 15
- key_gain: float32 [96], replicated, may hold values from 0.5 to 15
- output_gain: float32 [512], replicated, may hold values from 0.1 to 1.9
- output_weight: bfloat16 [512, 2048], P(None, 'tp'), may hold values from -0.25 to 0.25
Outputs:
- layer_output: bfloat16 [1024, 2048], P('sp', 'tp')
- log_totals: float32 [8, 1024], P('tp', 'sp')
Inputs may be any that keep to these rules, and one draw needn't show every extreme that they name: `doc_lengths`: the lengths sum to 1024; the longest is exactly 640.
All inputs are finite; a program needn't handle non-finite values.
Results may differ from a plain program's by a relative error of at most 0.019.
The roundings to bfloat16 on the way count: a program that leaves them out, or rounds other values in their place, can miss the bound.
Values may be sent and summed in bfloat16 or wider, within the bound.
A program may use at most 64 MiB of HBM per device.

v0:
```python
import math

import jax
import jax.numpy as jnp
from jax import lax
from jax.sharding import PartitionSpec as P

NOPE = 64
ROPE = 32
VD = 64


EPS = 1e-06
THETA = 10000.0
NEG = -1e30
key_span = 2048


def norm_rows(matrix, scaling):
    mean_square = jnp.mean(matrix * matrix, axis=-1, keepdims=True)
    return matrix * lax.rsqrt(mean_square + EPS) * scaling


def rotate(matrix, places):
    half_width = matrix.shape[-1] // 2
    inverse = THETA ** (-jnp.arange(half_width, dtype=jnp.float32) / half_width)
    angles = places.astype(jnp.float32)[:, None, None] * inverse
    cosine = jnp.cos(angles)
    sine_part = jnp.sin(angles)
    leading = matrix[..., :half_width]
    trailing = matrix[..., half_width:]
    return jnp.concatenate(
        [leading * cosine - trailing * sine_part, trailing * cosine + leading * sine_part], axis=-1
    )


def doc_index(places, doc_ends):
    return jnp.sum((places[:, None] >= doc_ends[None, :]).astype(jnp.int32), axis=1)


def head_keys(latent_rows, rope_rows, places, key_up, value_up, key_gain):
    row_count = latent_rows.shape[0]
    head_count = key_up.shape[1] // NOPE
    plain_part = jnp.dot(latent_rows, key_up, preferred_element_type=jnp.float32).reshape(
        row_count, head_count, NOPE
    )
    shared_part = jnp.broadcast_to(
        rope_rows.astype(jnp.float32)[:, None, :], (row_count, head_count, ROPE)
    )
    joined = norm_rows(jnp.concatenate([plain_part, shared_part], axis=-1), key_gain)
    key_block = jnp.concatenate(
        [joined[..., :NOPE], rotate(joined[..., NOPE:], places)], axis=-1
    ).astype(jnp.bfloat16)
    value_block = jnp.dot(latent_rows, value_up, preferred_element_type=jnp.float32).astype(
        jnp.bfloat16
    )
    return (key_block, value_block.reshape(row_count, head_count, VD))


def absorb_block(running, queries, query_docs, key_block, value_block, key_docs, score_scale):
    row_top, row_total, weighted = running
    scores = (
        jnp.einsum("qhd,khd->hqk", queries, key_block, preferred_element_type=jnp.float32)
        * score_scale
    )
    allowed = (query_docs[:, None] == key_docs[None, :])[None]
    scores = jnp.where(allowed, scores, NEG)
    newest_top = jnp.maximum(row_top, jnp.max(scores, axis=-1))
    weights = jnp.where(allowed, jnp.exp(scores - newest_top[..., None]), 0.0)
    rescale = jnp.exp(row_top - newest_top)
    row_total = row_total * rescale + jnp.sum(weights, axis=-1)
    update = jnp.einsum(
        "hqk,khd->qhd",
        weights.astype(jnp.bfloat16),
        value_block,
        preferred_element_type=jnp.float32,
    )
    weighted = weighted * jnp.transpose(rescale)[:, :, None] + update
    return (newest_top, row_total, weighted)


def per_device(
    tokens,
    doc_lengths,
    query_down,
    latent_down,
    rope_down,
    query_latent_gain,
    latent_gain,
    query_up,
    key_up,
    value_up,
    query_gain,
    key_gain,
    output_gain,
    output_weight,
):
    query_latent = norm_rows(
        jnp.dot(tokens, query_down, preferred_element_type=jnp.float32), query_latent_gain
    ).astype(jnp.bfloat16)
    key_latent = norm_rows(
        jnp.dot(tokens, latent_down, preferred_element_type=jnp.float32), latent_gain
    ).astype(jnp.bfloat16)
    rope_key = jnp.dot(tokens, rope_down, preferred_element_type=jnp.float32).astype(jnp.bfloat16)
    query_rows, latent_rows, rope_rows = (
        lax.all_gather(query_latent, "tp", axis=0, tiled=True),
        lax.all_gather(key_latent, "tp", axis=0, tiled=True),
        lax.all_gather(rope_key, "tp", axis=0, tiled=True),
    )
    row_count = query_rows.shape[0]
    head_width = NOPE + ROPE
    head_count = query_up.shape[1] // head_width
    row_offset = lax.axis_index("sp") * row_count
    places = row_offset + jnp.arange(row_count, dtype=jnp.int32)
    doc_ends = jnp.cumsum(doc_lengths)
    query_docs = doc_index(places, doc_ends)
    lowest_doc = query_docs[0]
    highest_doc = query_docs[row_count - 1]
    query_raw = jnp.dot(query_rows, query_up, preferred_element_type=jnp.float32).reshape(
        row_count, head_count, head_width
    )
    query_raw = norm_rows(query_raw, query_gain)
    queries = jnp.concatenate(
        [query_raw[..., :NOPE], rotate(query_raw[..., NOPE:], places)], axis=-1
    ).astype(jnp.bfloat16)
    score_scale = head_width ** (-0.5)
    initial = (
        jnp.full((head_count, row_count), NEG, jnp.float32),
        jnp.zeros((head_count, row_count), jnp.float32),
        jnp.zeros((row_count, head_count, VD), jnp.float32),
    )

    def from_latent(sliced, key_places):
        return head_keys(sliced[0], sliced[1], key_places, key_up, value_up, key_gain)

    pieces = (
        lax.all_gather(latent_rows, "sp", axis=0, tiled=True),
        lax.all_gather(rope_rows, "sp", axis=0, tiled=True),
    )
    piece_rows = pieces[0].shape[0]
    span_rows = math.gcd(piece_rows, key_span)

    def one_span(turn_index, carried):
        offset = turn_index * span_rows
        sliced = tuple(
            (lax.dynamic_slice_in_dim(member, offset, span_rows, 0) for member in pieces)
        )
        key_places = offset + jnp.arange(span_rows, dtype=jnp.int32)
        key_docs = doc_index(key_places, doc_ends)
        touches = (key_docs[0] <= highest_doc) & (key_docs[span_rows - 1] >= lowest_doc)

        def absorb_span(current):
            key_block, value_block = from_latent(sliced, key_places)
            return absorb_block(
                current, queries, query_docs, key_block, value_block, key_docs, score_scale
            )

        def pass_over(current):
            return current

        return lax.cond(touches, absorb_span, pass_over, carried)

    row_top, row_total, weighted = lax.fori_loop(0, piece_rows // span_rows, one_span, initial)
    head_out = (
        (weighted / jnp.transpose(row_total)[:, :, None])
        .astype(jnp.bfloat16)
        .reshape(row_count, head_count * VD)
    )
    log_totals = row_top + jnp.log(row_total)
    every_head = lax.all_gather(head_out, "tp", axis=1, tiled=True)
    normed = norm_rows(every_head.astype(jnp.float32), output_gain).astype(jnp.bfloat16)
    layer_output = jnp.dot(normed, output_weight, preferred_element_type=jnp.float32).astype(
        jnp.bfloat16
    )
    return (layer_output, log_totals)


def solution(mesh):
    return jax.shard_map(
        per_device,
        mesh=mesh,
        in_specs=(
            P(("sp", "tp"), None),
            P(),
            P(),
            P(),
            P(),
            P(),
            P(),
            P(None, "tp"),
            P(None, "tp"),
            P(None, "tp"),
            P(),
            P(),
            P(),
            P(None, "tp"),
        ),
        out_specs=(P("sp", "tp"), P("tp", "sp")),
        check_vma=False,
    )
```

profile of v0, /device:TPU:0, one launch (start us, length us, event | category | flops | bytes accessed | tf_op | source)
XLA Modules:
  0.0 103.3 jit_solution(12043495153674618477)
XLA Ops:
  0.6 0.0 copy-start
  0.6 0.0 copy-start.1
  0.7 0.0 copy-start.9
  0.7 1.7 %copy-done = bf16[2048,512]{1,0:T(8,128)(2,1)S(1)} copy-done((bf16[2048,512]{1,0:T(8,128)(2,1)S(1)}, bf16[2048,512]{1,0:T(8,128)(2,1)}, u32[]{:S(2)}) %copy-start) | copy-done | bytes 2097176
  2.4 1.5 %multiply_reduce_fusion.2 = (f32[32]{0:T(128)S(1)}, f32[32,512]{1,0:T(8,128)S(1)}) fusion(bf16[32,2048]{1,0:T(8,128)(2,1)} %param.16, bf16[2048,512]{1,0:T(8,128)(2,1)S(1)} %copy-done), kind=kOutput, calls=%fused_computation.49 | convolution fusion | flops 67141600 | bytes 2293888 | tf_op jit(solution)/shard_map/dot_general | solution.py:99
  3.8 0.0 copy-start.3
  3.9 0.0 copy-start.4
  3.9 0.0 copy-done.9
  3.9 0.1 multiply_convert_fusion
  4.0 6.5 %all_gather.22 = bf16[128,512]{1,0:T(8,128)(2,1)S(1)} all-gather(bf16[32,512]{1,0:T(8,128)(2,1)S(1)} %multiply_convert_fusion), channel_id=1, replica_groups=mesh['sp'=8,'tp'=4] {'tp'}, dimensions={0}, use_global_device_ids=true | all-gather | bytes 163840 | tf_op jit(solution)/shard_map/all_gather | solution.py:106
  10.5 0.2 fusion.28
  10.7 0.1 multiply_multiply_fusion.1
  10.8 0.1 multiply_cosine_fusion.2
  11.0 0.6 pad_maximum_fusion.1
  11.6 0.0 copy-done.12
  11.6 0.1 copy.29
  11.8 0.1 reduce
  11.9 0.1 convert_reduce_fusion.1
  12.0 1.6 %multiply_reduce_fusion.3 = (f32[32]{0:T(128)S(1)}, f32[32,256]{1,0:T(8,128)S(1)}) fusion(bf16[32,2048]{1,0:T(8,128)(2,1)S(1)} %copy-done.1, bf16[2048,256]{1,0:T(8,128)(2,1)} %param.19), kind=kOutput, calls=%fused_computation.54 | convolution fusion | flops 33570784 | bytes 1212544 | tf_op jit(solution)/shard_map/dot_general | solution.py:102
  13.6 0.1 multiply_convert_fusion.1
  13.7 5.4 %all_gather.18 = bf16[128,256]{1,0:T(8,128)(2,1)S(1)} all-gather(bf16[32,256]{1,0:T(8,128)(2,1)S(1)} %multiply_convert_fusion.1), channel_id=1, replica_groups=mesh['sp'=8,'tp'=4] {'tp'}, dimensions={0}, use_global_device_ids=true | all-gather | bytes 81920 | tf_op jit(solution)/shard_map/all_gather | solution.py:107
  19.1 32.1 %all_gather.19 = bf16[1024,256]{1,0:T(8,128)(2,1)S(1)} all-gather(bf16[128,256]{1,0:T(8,128)(2,1)S(1)} %all_gather.18), channel_id=1, replica_groups=mesh['sp'=8,'tp'=4] {'sp'}, dimensions={0}, use_global_device_ids=true | all-gather | bytes 589824 | tf_op jit(solution)/shard_map/all_gather | solution.py:137
  51.2 0.1 convert_reduce_fusion
  51.3 0.0 copy-done.3
  51.3 0.2 convolution_convert_fusion.2
  51.4 5.2 %all_gather.20 = bf16[128,32]{1,0:T(8,128)(2,1)S(1)} all-gather(bf16[32,32]{1,0:T(8,128)(2,1)S(1)} %convolution_convert_fusion.2), channel_id=1, replica_groups=mesh['sp'=8,'tp'=4] {'tp'}, dimensions={0}, use_global_device_ids=true | all-gather | bytes 10240 | tf_op jit(solution)/shard_map/all_gather | solution.py:108
  56.6 30.7 %all_gather.21 = bf16[1024,32]{1,0:T(8,128)(2,1)S(1)} all-gather(bf16[128,32]{1,0:T(8,128)(2,1)S(1)} %all_gather.20), channel_id=1, replica_groups=mesh['sp'=8,'tp'=4] {'sp'}, dimensions={0}, use_global_device_ids=true | all-gather | bytes 73728 | tf_op jit(solution)/shard_map/all_gather | solution.py:138
  87.4 0.6 fusion.25
  90.5 4.6 %conditional.1 = (f32[2,128]{1,0:T(2,128)S(1)}, f32[128,2,64]{0,2,1:T(8,128)S(1)}, f32[2,128]{1,0:T(2,128)S(1)}) conditional(s32[]{:T(128)} %bitcast.1, (f32[2,128]{1,0:T(2,128)S(1)}, f32[2,128]{1,0:T(2,128)S(1)}, f32[128,2,64]{0,2,1:T(8,128)S(1)}) %tuple.27, (s32[128]{0:T(128)S(1)}, s32[1024]{0:T(1024)S(1)}, ...), branch_computations={%region_6.7_spmd.clone, %region_7.11_spmd.clone} | conditional | flops 223451936 | bytes 11297928 | solution.py:161
  90.6 0.6 copy-done.7
  91.1 0.3 fusion.27
  91.5 0.1 copy.30
  91.6 0.0 copy-start.6
  91.6 0.1 multiply_reduce_fusion
  91.7 0.8 multiply_multiply_fusion
  92.5 0.0 copy-start.5
  92.6 0.9 multiply_cosine_fusion.1
  93.6 0.0 copy-done.8
  93.6 0.2 broadcast_compare_fusion
  93.8 0.4 fusion.24
  94.2 0.0 copy-done.5
  94.2 0.3 convolution_convert_fusion
  94.5 0.4 fusion.2
  94.9 0.2 fusion.4
  95.2 0.6 log_add_fusion
  95.8 5.4 %all_gather.23 = bf16[128,512]{0,1:T(8,128)(2,1)S(1)} all-gather(bf16[128,128]{0,1:T(8,128)(2,1)S(1)} %bitcast.37), channel_id=1, replica_groups=mesh['sp'=8,'tp'=4] {'tp'}, dimensions={1}, use_global_device_ids=true | all-gather | bytes 163840 | tf_op jit(solution)/shard_map/all_gather | solution.py:170
  101.2 0.1 fusion.17
  101.3 2.1 %convolution_convert_fusion.1 = bf16[128,512]{1,0:T(8,128)(2,1)} fusion(bf16[512,512]{1,0:T(8,128)(2,1)} %param.29, bf16[128,512]{0,1:T(8,128)(2,1)S(1)} %all_gather.23, f32[512]{0:T(512)} %param.28, f32[128]{0:T(128)S(1)} %add_rsqrt_fusion.2), kind=kOutput, calls=%fused_computation.35 | convolution fusion | flops 67436544 | bytes 788992 | tf_op jit(solution)/shard_map/dot_general | solution.py:172
  (40 shorter events, 0.3 us)
Async XLA Ops:
  0.6 1.7 %copy-start = (bf16[2048,512]{1,0:T(8,128)(2,1)S(1)}, bf16[2048,512]{1,0:T(8,128)(2,1)}, u32[]{:S(2)}) copy-start(bf16[2048,512]{1,0:T(8,128)(2,1)} %param.18) | copy-start | bytes 6291460
  0.6 11.3 %copy-start.1 = (bf16[32,2048]{1,0:T(8,128)(2,1)S(1)}, bf16[32,2048]{1,0:T(8,128)(2,1)}, u32[]{:S(2)}) copy-start(bf16[32,2048]{1,0:T(8,128)(2,1)} %param.16) | copy-start | bytes 393220
  0.7 3.2 %copy-start.9 = (f32[512]{0:T(512)S(1)}, f32[512]{0:T(512)}, u32[]{:S(2)}) copy-start(f32[512]{0:T(512)} %param.21) | copy-start | bytes 6148
  0.7 9.8 %copy-start.2 = (bf16[512,192]{0,1:T(8,128)(2,1)S(1)}, bf16[512,192]{0,1:T(8,128)(2,1)}, u32[]{:S(2)}) copy-start(bf16[512,192]{0,1:T(8,128)(2,1)} %param.23) | copy-start | bytes 589828
  0.7 10.1 %copy-start.11 = (f32[96]{0:T(128)S(1)}, f32[96]{0:T(128)}, u32[]{:S(2)}) copy-start(f32[96]{0:T(128)} %param.26) | copy-start | bytes 1156
  0.7 10.9 %copy-start.12 = (s32[16]{0:T(128)S(1)}, s32[16]{0:T(128)}, u32[]{:S(2)}) copy-start(s32[16]{0:T(128)} %param.17) | copy-start | bytes 196
  0.7 12.9 %copy-start.10 = (f32[256]{0:T(256)S(1)}, f32[256]{0:T(256)}, u32[]{:S(2)}) copy-start(f32[256]{0:T(256)} %param.22) | copy-start | bytes 3076
  3.8 47.4 %copy-start.3 = (bf16[2048,32]{0,1:T(8,128)(2,1)S(1)}, bf16[2048,32]{0,1:T(8,128)(2,1)}, u32[]{:S(2)}) copy-start(bf16[2048,32]{0,1:T(8,128)(2,1)} %param.20) | copy-start | bytes 393220
  3.9 86.7 %copy-start.4 = (bf16[256,128]{1,0:T(8,128)(2,1)S(1)}, bf16[256,128]{1,0:T(8,128)(2,1)}, u32[]{:S(2)}) copy-start(bf16[256,128]{1,0:T(8,128)(2,1)} %param.24) | copy-start | bytes 196612
  90.6 0.6 copy-start.7
  91.6 2.0 %copy-start.8 = (s32[128]{0:T(128)S(1)}, s32[128]{0:T(128)}, u32[]{:S(2)}) copy-start(s32[128]{0:T(128)} %copy-done.7) | copy-start | bytes 1540 | tf_op jit(solution)/shard_map/while/body/eval_jaxpr/cond
  91.6 2.2 %copy-start.6 = (bf16[128,2,96]{0,2,1:T(8,128)(2,1)S(1)}, bf16[128,2,96]{0,2,1:T(8,128)(2,1)}, u32[]{:S(2)}) copy-start(bf16[128,2,96]{0,2,1:T(8,128)(2,1)} %get-tuple-element.141) | copy-start | bytes 147460 | tf_op jit(solution)/shard_map/while/body/eval_jaxpr/cond
  92.5 1.7 %copy-start.5 = (bf16[256,128]{1,0:T(8,128)(2,1)S(1)}, bf16[256,128]{1,0:T(8,128)(2,1)}, u32[]{:S(2)}) copy-start(bf16[256,128]{1,0:T(8,128)(2,1)} %get-tuple-element.146) | copy-start | bytes 196612 | tf_op jit(solution)/shard_map/while/body/eval_jaxpr/cond
where the time goes:
time: 104 us; the launch traced here: 103 us
  blocking collectives  85.3 us (82%)
  matrix products  6.87 us (7%)
  other arithmetic  4.36 us (4%)
  between operations  3.4 us (3%)
  local copies, waits for them, and re-layouts  3.18 us (3%)
    all_gather x1, blocking collectives, per_device(): lax.all_gather(latent_rows, 'sp', axis=0, tiled=True)  32.1 us
    all_gather x1, blocking collectives, per_device(): lax.all_gather(rope_rows, 'sp', axis=0, tiled=True)  30.7 us
    all_gather x1, blocking collectives, per_device(): lax.all_gather(query_latent, 'tp', axis=0, tiled=True)  6.49 us
    all_gather x1, blocking collectives, per_device(): every_head = lax.all_gather(head_out, 'tp', axis=1, tiled=True)  5.42 us
    all_gather x1, blocking collectives, per_device(): lax.all_gather(key_latent, 'tp', axis=0, tiled=True)  5.39 us
    all_gather x1, blocking collectives, per_device(): lax.all_gather(rope_key, 'tp', axis=0, tiled=True)  5.19 us

commit v1 on v0

v1 whole, which is shorter than its diff:
```python
import functools

import jax
import jax.numpy as jnp
import numpy as np
from jax import lax
from jax.experimental import pallas as pl
from jax.experimental.pallas import tpu as pltpu
from jax.sharding import PartitionSpec as P

NOPE = 64
ROPE = 32
VD = 64
WIDTH = NOPE + ROPE
LANES = 128

EPS = 1e-06
THETA = 10000.0
NEG = -1e30
KEY_CHUNK = 1024
F32 = jnp.float32
BF16 = jnp.bfloat16
MESH = pl.DeviceIdType.MESH


def each(count, body):
    if count <= 16:
        for step in range(count):
            body(step)
    else:
        lax.fori_loop(0, count, lambda step, _: (body(step), 0)[1], 0)


def nt_dot(left, right):
    return lax.dot_general(left, right, (((1,), (1,)), ((), ())), preferred_element_type=F32)


def norm_lanes(matrix, scaling):
    mean_square = jnp.mean(matrix * matrix, axis=-1, keepdims=True)
    return matrix * lax.rsqrt(mean_square + EPS) * scaling


def column(row):
    width = row.shape[1]
    full = jnp.broadcast_to(row, (LANES, width))
    full = jnp.concatenate([full, jnp.zeros((LANES, LANES - width), F32)], axis=1)
    return jnp.transpose(full)[:width, 0:1]


def rotated(part, cosine, sine):
    half = part.shape[0] // 2
    leading, trailing = part[:half], part[half:]
    return jnp.concatenate(
        [leading * cosine - trailing * sine, trailing * cosine + leading * sine], axis=0
    )


def xor(index, bits):
    return jnp.bitwise_xor(index, bits)


def kernel(
    n_sp, n_tp,
    tokens_hbm, lengths_hbm, query_down_hbm, latent_down_hbm, rope_down_hbm,
    query_latent_gain_hbm, latent_gain_hbm, query_up_hbm, key_up_hbm, value_up_hbm,
    query_gain_hbm, key_gain_hbm, output_gain_hbm, output_weight_hbm, inverse_hbm,
    out_ref, log_ref,
    tokens, lengths, query_down, latent_down, rope_down,
    query_latent_gain, latent_gain, query_up, key_up, value_up,
    query_gain, key_gain, output_gain, output_weight, inverse_ref,
    lat, qlat, heads, load_sem,
    z_send, z_recv, a_send, a_recv, b_send, b_recv, c_send, c_recv,
    q_send, q_recv, h_send, h_recv,
):
    sp, tp = lax.axis_index("sp"), lax.axis_index("tp")
    n_outer = n_sp // 2
    rows = tokens.shape[0]
    group_rows = rows * n_tp
    kvr = latent_down.shape[1]
    head_count = key_up.shape[1] // NOPE
    out_width = head_count * VD

    loads = [
        pltpu.make_async_copy(source, target, load_sem.at[position])
        for position, (source, target) in enumerate((
            (tokens_hbm, tokens), (latent_down_hbm, latent_down), (rope_down_hbm, rope_down),
            (latent_gain_hbm, latent_gain), (query_down_hbm, query_down),
            (query_latent_gain_hbm, query_latent_gain), (lengths_hbm, lengths),
            (query_gain_hbm, query_gain), (key_gain_hbm, key_gain), (inverse_hbm, inverse_ref),
            (query_up_hbm, query_up), (key_up_hbm, key_up), (value_up_hbm, value_up),
            (output_gain_hbm, output_gain), (output_weight_hbm, output_weight),
        ))
    ]
    for load in loads:
        load.start()

    barrier = pltpu.get_barrier_semaphore()

    def greet(step):
        pl.semaphore_signal(
            barrier, inc=1, device_id=(xor(sp, 2 * (step + 1)), tp), device_id_type=MESH
        )

    each(n_outer - 1, greet)
    pl.semaphore_signal(barrier, inc=1, device_id=(xor(sp, 1), tp), device_id_type=MESH)
    for other in range(1, n_tp):
        pl.semaphore_signal(barrier, inc=1, device_id=(sp, xor(tp, other)), device_id_type=MESH)

    parity = lax.rem(tp, 2)
    first = (xor(sp, 1 - parity), xor(tp, 2 * parity))
    second = (xor(sp, parity), xor(tp, 2 * (1 - parity)))
    core = (sp, xor(tp, 1))

    def block(device):
        start = pl.multiple_of((device[0] * n_tp + device[1]) * rows, rows)
        return lat.at[pl.ds(start, rows)]

    def send(ref, sends, recvs, index, target):
        copy = pltpu.make_async_remote_copy(
            src_ref=ref, dst_ref=ref, send_sem=sends.at[index], recv_sem=recvs.at[index],
            device_id=target, device_id_type=MESH,
        )
        copy.start()
        return copy

    def along(device, step):
        return (xor(device[0], 2 * step), device[1])

    me = (sp, tp)
    for load in loads[:4]:
        load.wait()
    latent = jnp.dot(tokens[...], latent_down[...], preferred_element_type=F32)
    rope = jnp.dot(tokens[...], rope_down[...], preferred_element_type=F32)
    latent = norm_lanes(latent, latent_gain[...]).astype(BF16)
    rope = jnp.concatenate([rope, jnp.zeros((rows, LANES - ROPE), F32)], axis=1).astype(BF16)
    own = pl.ds(pl.multiple_of((sp * n_tp + tp) * rows, rows), rows)
    lat[own, :kvr] = latent
    lat[own, kvr:] = rope
    pl.semaphore_wait(barrier, n_outer + n_tp - 1)

    each(n_outer - 1, lambda k: send(block(me), z_send, z_recv, k, along(me, k + 1)) and None)
    send(block(me), a_send, a_recv, 0, first)
    send(block(me), b_send, b_recv, 0, second)
    send(block(me), c_send, c_recv, 0, core)

    for load in loads[4:6]:
        load.wait()
    query_latent = jnp.dot(tokens[...], query_down[...], preferred_element_type=F32)
    query_latent = norm_lanes(query_latent, query_latent_gain[...]).astype(BF16)
    own_q = pl.ds(pl.multiple_of(tp * rows, rows), rows)
    qlat[own_q, :] = query_latent
    for other in range(1, n_tp):
        send(qlat.at[own_q], q_send, q_recv, other - 1, (sp, xor(tp, other)))

    for load in loads[6:]:
        load.wait()
    inverse = inverse_ref[...]
    query_gain_column = column(query_gain[...])
    key_gain_column = column(key_gain[...])
    ends = []
    total = 0
    for doc in range(lengths.shape[0]):
        total = total + lengths[doc]
        ends.append(total)

    def docs_of(places):
        found = jnp.zeros(places.shape, jnp.int32)
        for end in ends:
            found = found + (places >= end).astype(jnp.int32)
        return found

    seq = lat.shape[0]
    span = min(seq, KEY_CHUNK)
    query_base = sp * group_rows
    query_places = query_base + lax.broadcasted_iota(jnp.int32, (1, group_rows), 1)
    query_angles = inverse * query_places.astype(F32)
    query_cos, query_sin = jnp.cos(query_angles), jnp.sin(query_angles)
    query_docs = docs_of(query_base + lax.broadcasted_iota(jnp.int32, (group_rows, 1), 0))

    def key_tables(offset):
        places = offset + lax.broadcasted_iota(jnp.int32, (1, span), 1)
        angles = inverse * places.astype(F32)
        return jnp.cos(angles), jnp.sin(angles), docs_of(places) == query_docs

    plain_rows = head_count * NOPE
    key_up_t = jnp.transpose(key_up[...].astype(F32)).astype(BF16)
    eye = (
        lax.broadcasted_iota(jnp.int32, (ROPE, LANES), 0)
        == lax.broadcasted_iota(jnp.int32, (ROPE, LANES), 1)
    ).astype(F32).astype(BF16)
    if seq == span:
        tables = key_tables(0)

    def recv(ref, sends, recvs, index, target):
        pltpu.make_async_remote_copy(
            src_ref=ref, dst_ref=ref, send_sem=sends.at[index], recv_sem=recvs.at[index],
            device_id=target, device_id_type=MESH,
        ).wait_recv()

    def from_first(k):
        source = along(first, k)
        recv(block(source), a_send, a_recv, k, first)
        send(block(source), b_send, b_recv, 2 * k + 1, second)
        send(block(source), c_send, c_recv, 4 * k + 1, core)

    def from_z(k):
        source = along(me, k)
        recv(block(source), z_send, z_recv, k - 1, source)
        send(block(source), a_send, a_recv, k, first)
        send(block(source), b_send, b_recv, 2 * k, second)
        send(block(source), c_send, c_recv, 4 * k, core)

    def both(k):
        return along((xor(sp, 1), xor(tp, 2)), k)

    def from_second(k):
        source = along(second, k)
        recv(block(source), b_send, b_recv, 2 * k, second)
        send(block(source), c_send, c_recv, 4 * k + 2, core)

    def from_both(k):
        source = both(k)
        recv(block(source), b_send, b_recv, 2 * k + 1, second)
        send(block(source), c_send, c_recv, 4 * k + 3, core)

    from_first(0)
    from_second(0)
    each(n_outer - 1, lambda k: from_z(k + 1))
    from_both(0)

    def rest(k):
        from_first(k + 1)
        from_second(k + 1)

    each(n_outer - 1, rest)

    for other in range(1, n_tp):
        peer = xor(tp, other)
        rows_of = pl.ds(pl.multiple_of(peer * rows, rows), rows)
        recv(qlat.at[rows_of], q_send, q_recv, other - 1, (sp, peer))
    raw = jnp.dot(qlat[...], query_up[...], preferred_element_type=F32)
    queries = []
    for head in range(head_count):
        piece = raw[:, head * WIDTH:(head + 1) * WIDTH]
        piece = jnp.concatenate([piece, jnp.zeros((group_rows, LANES - WIDTH), F32)], axis=1)
        piece = jnp.transpose(piece)[:WIDTH]
        scale = lax.rsqrt(jnp.mean(piece * piece, axis=0, keepdims=True) + EPS)
        piece = piece * scale * query_gain_column
        piece = jnp.concatenate(
            [piece[:NOPE], rotated(piece[NOPE:], query_cos, query_sin),
             jnp.zeros((LANES - WIDTH, group_rows), F32)], axis=0
        )
        queries.append(jnp.transpose(piece)[:, :WIDTH].astype(BF16))

    each(n_outer - 1, lambda k: from_both(k + 1))

    def from_core(k):
        recv(block(along(core, k)), c_send, c_recv, 4 * k, core)
        partner_first = (xor(core[0], parity), xor(core[1], 2 * (1 - parity)))
        partner_second = (xor(core[0], 1 - parity), xor(core[1], 2 * parity))
        recv(block(along(partner_first, k)), c_send, c_recv, 4 * k + 1, core)
        recv(block(along(partner_second, k)), c_send, c_recv, 4 * k + 2, core)
        recv(block(along((xor(core[0], 1), xor(core[1], 2)), k)), c_send, c_recv, 4 * k + 3, core)

    each(n_outer, from_core)

    lane = lax.broadcasted_iota(jnp.int32, (group_rows, out_width), 1)
    score_scale = WIDTH ** (-0.5)

    def absorb(offset, known, carried):
        cosine, sine, allowed = known
        block_rows = lat[pl.ds(offset, span), :]
        latents = block_rows[:, :kvr]
        plain = nt_dot(key_up_t, latents)
        shared = nt_dot(eye, block_rows[:, kvr:])
        values = jnp.dot(latents, value_up[...], preferred_element_type=F32).astype(BF16)
        shared_square = jnp.sum(shared * shared, axis=0, keepdims=True)
        fresh = []
        for head in range(head_count):
            top, row_total, weighted = carried[head]
            part = plain[head * NOPE:(head + 1) * NOPE]
            square = jnp.sum(part * part, axis=0, keepdims=True) + shared_square
            scale = lax.rsqrt(square * (1.0 / WIDTH) + EPS)
            tail = rotated(shared * scale * key_gain_column[NOPE:], cosine, sine)
            keys = jnp.concatenate(
                [part * scale * key_gain_column[:NOPE], tail], axis=0
            ).astype(BF16)
            scores = jnp.dot(queries[head], keys, preferred_element_type=F32) * score_scale
            scores = jnp.where(allowed, scores, NEG)
            newest = jnp.maximum(top, jnp.max(scores, axis=1, keepdims=True))
            weights = jnp.where(allowed, jnp.exp(scores - newest), 0.0)
            rescale = jnp.exp(top - newest)
            row_total = row_total * rescale + jnp.sum(weights, axis=1, keepdims=True)
            weighted = weighted * rescale + jnp.dot(
                weights.astype(BF16), values, preferred_element_type=F32
            )
            fresh.append((newest, row_total, weighted))
        return tuple(fresh)

    carried = tuple(
        (jnp.full((group_rows, 1), NEG, F32), jnp.zeros((group_rows, 1), F32),
         jnp.zeros((group_rows, out_width), F32))
        for _ in range(head_count)
    )
    if seq == span:
        carried = absorb(0, tables, carried)
    else:
        def one_chunk(turn, held):
            offset = pl.multiple_of(turn * span, span)
            return absorb(offset, key_tables(offset), held)

        carried = lax.fori_loop(0, seq // span, one_chunk, carried)

    head_out = jnp.zeros((group_rows, out_width), F32)
    for head in range(head_count):
        top, row_total, weighted = carried[head]
        inside = (lane >= head * VD) & (lane < (head + 1) * VD)
        head_out = jnp.where(inside, weighted / row_total, head_out)
    heads[tp] = head_out.astype(BF16)
    for other in range(1, n_tp):
        send(heads.at[tp], h_send, h_recv, other - 1, (sp, xor(tp, other)))

    logs = jnp.concatenate(
        [jnp.broadcast_to(top + jnp.log(row_total), (group_rows, LANES // head_count))
         for top, row_total, _ in carried], axis=1
    )
    logs = jnp.transpose(logs)
    for head in range(head_count):
        start = head * (LANES // head_count)
        log_ref[head:head + 1, :] = logs[start:start + 1]

    for other in range(1, n_tp):
        peer = xor(tp, other)
        recv(heads.at[peer], h_send, h_recv, other - 1, (sp, peer))
    pieces = [heads[index].astype(F32) for index in range(n_tp)]
    square = sum(jnp.sum(piece * piece, axis=1, keepdims=True) for piece in pieces)
    scale = lax.rsqrt(square * (1.0 / (n_tp * out_width)) + EPS)
    normed = jnp.concatenate(
        [(piece * scale * output_gain[:, index * out_width:(index + 1) * out_width]).astype(BF16)
         for index, piece in enumerate(pieces)], axis=1
    )
    out_ref[...] = jnp.dot(normed, output_weight[...], preferred_element_type=F32).astype(BF16)

    def sent(ref, sends, recvs, index):
        pltpu.make_async_remote_copy(
            src_ref=ref, dst_ref=ref, send_sem=sends.at[index], recv_sem=recvs.at[index],
            device_id=core, device_id_type=MESH,
        ).wait_send()

    each(n_outer - 1, lambda k: sent(block(me), z_send, z_recv, k))
    each(n_outer, lambda k: sent(block(along(me, k)), a_send, a_recv, k))

    def sent_rest(k):
        sent(block(along(me, k)), b_send, b_recv, 2 * k)
        sent(block(along(first, k)), b_send, b_recv, 2 * k + 1)
        sent(block(along(me, k)), c_send, c_recv, 4 * k)
        sent(block(along(first, k)), c_send, c_recv, 4 * k + 1)
        sent(block(along(second, k)), c_send, c_recv, 4 * k + 2)
        sent(block(both(k)), c_send, c_recv, 4 * k + 3)

    each(n_outer, sent_rest)
    for other in range(n_tp - 1):
        sent(qlat.at[own_q], q_send, q_recv, other)
        sent(heads.at[tp], h_send, h_recv, other)


def per_device(
    n_sp, n_tp, tokens, doc_lengths, query_down, latent_down, rope_down,
    query_latent_gain, latent_gain, query_up, key_up, value_up,
    query_gain, key_gain, output_gain, output_weight,
):
    rows = tokens.shape[0]
    group_rows = rows * n_tp
    seq = group_rows * n_sp
    half = ROPE // 2
    inverse = jnp.asarray(
        np.float32(THETA) ** (-np.arange(half, dtype=np.float32) / half), F32
    ).reshape(half, 1)
    operands = (
        tokens, doc_lengths, query_down, latent_down, rope_down,
        query_latent_gain[None], latent_gain[None], query_up, key_up, value_up,
        query_gain[None], key_gain[None], output_gain[None], output_weight, inverse,
    )
    n_outer = n_sp // 2
    head_count = key_up.shape[1] // NOPE
    kvr = latent_down.shape[1]
    held = [
        pltpu.SMEM(member.shape, member.dtype) if position == 1
        else pltpu.VMEM(member.shape, member.dtype)
        for position, member in enumerate(operands)
    ]
    dma = pltpu.SemaphoreType.DMA
    return pl.pallas_call(
        functools.partial(kernel, n_sp, n_tp),
        out_shape=(
            jax.ShapeDtypeStruct((group_rows, output_weight.shape[1]), BF16),
            jax.ShapeDtypeStruct((head_count, group_rows), F32),
        ),
        in_specs=[pl.BlockSpec(memory_space=pl.ANY)] * len(operands),
        out_specs=(pl.BlockSpec(memory_space=pltpu.VMEM),) * 2,
        scratch_shapes=held + [
            pltpu.VMEM((seq, kvr + LANES), BF16),
            pltpu.VMEM((group_rows, query_down.shape[1]), BF16),
            pltpu.VMEM((n_tp, group_rows, head_count * VD), BF16),
            dma((len(operands),)),
            dma((n_outer - 1,)), dma((n_outer - 1,)),
            dma((n_outer,)), dma((n_outer,)),
            dma((2 * n_outer,)), dma((2 * n_outer,)),
            dma((4 * n_outer,)), dma((4 * n_outer,)),
            dma((n_tp - 1,)), dma((n_tp - 1,)),
            dma((n_tp - 1,)), dma((n_tp - 1,)),
        ],
        compiler_params=pltpu.CompilerParams(
            collective_id=0, has_side_effects=True, vmem_limit_bytes=60 * 1024 * 1024
        ),
    )(*operands)


def solution(mesh):
    n_sp, n_tp = mesh.shape["sp"], mesh.shape["tp"]
    return jax.shard_map(
        functools.partial(per_device, n_sp, n_tp),
        mesh=mesh,
        in_specs=(
            P(("sp", "tp"), None), P(), P(), P(), P(), P(), P(),
            P(None, "tp"), P(None, "tp"), P(None, "tp"),
            P(), P(), P(), P(None, "tp"),
        ),
        out_specs=(P("sp", "tp"), P("tp", "sp")),
        check_vma=False,
    )
```

time: 104 us -> 30.1 us (0.29)
  blocking collectives: 85.3 us -> 0 us
  Pallas kernels: 0 us -> 22.8 us
  matrix products: 6.87 us -> 0 us
  other arithmetic: 4.36 us -> 0 us
  local copies, waits for them, and re-layouts: 3.18 us -> 6.46 us
  between operations: 3.4 us -> 0.64 us
    all_gather x6 -> x0, blocking collectives: 85.3 us -> none  [the longest x1 32.1 us: per_device(): lax.all_gather(latent_rows, 'sp', axis=0, tiled=True)]
    pallas_call x0 -> x1, Pallas kernels: none -> 22.8 us  [per_device(): pl.pallas_call(functools.partial(kernel, n_sp, n_tp), out_shape=(jax.Shap...]
    dot_general x9 -> x0, matrix products: 6.87 us -> none  [the longest x1 2.06 us: per_device(): jnp.dot(normed, output_weight, preferred_element_type=jnp.float32)]
    unnamed x18 -> x4, local copies, waits for them, and re-layouts: 1.71 us -> 6.46 us
where the time goes in v1:
time: 30.1 us; the launch traced here: 29.9 us
  Pallas kernels  22.8 us (76%)
  local copies, waits for them, and re-layouts  6.46 us (21%)
  between operations  0.64 us (2%)
    pallas_call x1, Pallas kernels, per_device(): pl.pallas_call(functools.partial(kernel, n_sp, n_tp), out_shape=(jax.Shap...  22.8 us
    unnamed x4, local copies, waits for them, and re-layouts  6.46 us

profile of v1, /device:TPU:0, one launch (start us, length us, event | category | flops | bytes accessed | tf_op | source)
XLA Modules:
  0.0 29.9 jit_solution(3535845746561769995)
XLA Ops:
  0.6 1.8 %copy.18.query_up_hbm = bf16[512,192]{1,0:T(8,128)(2,1)} copy(bf16[512,192]{0,1:T(8,128)(2,1)} %param.22) | data formatting | bytes 393216 | tf_op args[7]
  2.4 1.9 %copy.17.rope_down_hbm = bf16[2048,32]{1,0:T(8,128)(2,1)} copy(bf16[2048,32]{0,1:T(8,128)(2,1)} %param.19) | data formatting | bytes 262144 | tf_op args[4]
  4.3 22.8 %shard_map.158 = (bf16[128,512]{1,0:T(8,128)(2,1)}, f32[2,128]{1,0:T(2,128)}) custom-call(bf16[32,2048]{1,0:T(8,128)(2,1)} %tokens_hbm.1, s32[16]{0:T(128)} %lengths_hbm.1, bf16[2048,512]{1,0:T(8,128)(2,1)} %query_down_hbm.1, bf16[2048,256]{1,0:T(8,128)(2,1)} %latent_down_hbm.1, bf16[2048,32]{1,0:T(8,128)(2,1)} %copy.17.rope_down_hbm, f32[1,512]{1,0:T(1,128)} %bitcast.5, ...), custom_call_target="tpu_custom_call" | custom-call | tf_op jit(solution)/shard_map/pallas_call | solution.py:393
  27.1 1.6 %copy.21 = bf16[128,512]{1,0:T(8,128)(2,1)} copy(bf16[128,512]{1,0:T(8,128)(2,1)} %get-tuple-element.4) | data formatting | bytes 262144
  28.7 1.2 %copy.22 = f32[2,128]{1,0:T(2,128)} copy(f32[2,128]{1,0:T(2,128)} %get-tuple-element.5) | data formatting | bytes 2048

commit v2 on v1

--- a/solution.py
+++ b/solution.py
@@ -130,7 +130,7 @@
     for load in loads[:4]:
         load.wait()
     latent = jnp.dot(tokens[...], latent_down[...], preferred_element_type=F32)
-    rope = jnp.dot(tokens[...], rope_down[...], preferred_element_type=F32)
+    rope = nt_dot(tokens[...], rope_down[...])
     latent = norm_lanes(latent, latent_gain[...]).astype(BF16)
     rope = jnp.concatenate([rope, jnp.zeros((rows, LANES - ROPE), F32)], axis=1).astype(BF16)
     own = pl.ds(pl.multiple_of((sp * n_tp + tp) * rows, rows), rows)
@@ -149,8 +149,13 @@
     query_latent = norm_lanes(query_latent, query_latent_gain[...]).astype(BF16)
     own_q = pl.ds(pl.multiple_of(tp * rows, rows), rows)
     qlat[own_q, :] = query_latent
-    for other in range(1, n_tp):
-        send(qlat.at[own_q], q_send, q_recv, other - 1, (sp, xor(tp, other)))
+    across = (sp, xor(tp, 2))
+
+    def query_block(index):
+        return qlat.at[pl.ds(pl.multiple_of(index * rows, rows), rows)]
+
+    send(query_block(tp), q_send, q_recv, 0, across)
+    send(query_block(tp), q_send, q_recv, 1, core)
 
     for load in loads[6:]:
         load.wait()
@@ -225,6 +230,8 @@
 
     from_first(0)
     from_second(0)
+    recv(query_block(xor(tp, 2)), q_send, q_recv, 0, across)
+    send(query_block(xor(tp, 2)), q_send, q_recv, 2, core)
     each(n_outer - 1, lambda k: from_z(k + 1))
     from_both(0)
 
@@ -234,16 +241,12 @@
 
     each(n_outer - 1, rest)
 
-    for other in range(1, n_tp):
-        peer = xor(tp, other)
-        rows_of = pl.ds(pl.multiple_of(peer * rows, rows), rows)
-        recv(qlat.at[rows_of], q_send, q_recv, other - 1, (sp, peer))
-    raw = jnp.dot(qlat[...], query_up[...], preferred_element_type=F32)
+    recv(query_block(xor(tp, 1)), q_send, q_recv, 1, core)
+    recv(query_block(xor(tp, 3)), q_send, q_recv, 2, core)
+    raw = nt_dot(query_up[...], qlat[...])
     queries = []
     for head in range(head_count):
-        piece = raw[:, head * WIDTH:(head + 1) * WIDTH]
-        piece = jnp.concatenate([piece, jnp.zeros((group_rows, LANES - WIDTH), F32)], axis=1)
-        piece = jnp.transpose(piece)[:WIDTH]
+        piece = raw[head * WIDTH:(head + 1) * WIDTH]
         scale = lax.rsqrt(jnp.mean(piece * piece, axis=0, keepdims=True) + EPS)
         piece = piece * scale * query_gain_column
         piece = jnp.concatenate(
@@ -360,7 +363,7 @@
 
     each(n_outer, sent_rest)
     for other in range(n_tp - 1):
-        sent(qlat.at[own_q], q_send, q_recv, other)
+        sent(query_block(tp), q_send, q_recv, other)
         sent(heads.at[tp], h_send, h_recv, other)
 
 
@@ -377,8 +380,8 @@
         np.float32(THETA) ** (-np.arange(half, dtype=np.float32) / half), F32
     ).reshape(half, 1)
     operands = (
-        tokens, doc_lengths, query_down, latent_down, rope_down,
-        query_latent_gain[None], latent_gain[None], query_up, key_up, value_up,
+        tokens, doc_lengths, query_down, latent_down, rope_down.T,
+        query_latent_gain[None], latent_gain[None], query_up.T, key_up, value_up,
         query_gain[None], key_gain[None], output_gain[None], output_weight, inverse,
     )
     n_outer = n_sp // 2
@@ -396,7 +399,7 @@
             jax.ShapeDtypeStruct((group_rows, output_weight.shape[1]), BF16),
             jax.ShapeDtypeStruct((head_count, group_rows), F32),
         ),
-        in_specs=[pl.BlockSpec(memory_space=pl.ANY)] * len(operands),
+        in_specs=[pl.BlockSpec(memory_space=pltpu.HBM)] * len(operands),
         out_specs=(pl.BlockSpec(memory_space=pltpu.VMEM),) * 2,
         scratch_shapes=held + [
             pltpu.VMEM((seq, kvr + LANES), BF16),
@@ -411,9 +414,9 @@
             dma((n_tp - 1,)), dma((n_tp - 1,)),
         ],
         compiler_params=pltpu.CompilerParams(
-            collective_id=0, has_side_effects=True, vmem_limit_bytes=60 * 1024 * 1024
+            collective_id=0, has_side_effects=True, vmem_limit_bytes=(16 + seq // 512) * 1024 * 1024
         ),
-    )(*operands)
+    )(*[pltpu.with_memory_space_constraint(member, pltpu.HBM) for member in operands])
 
 
 def solution(mesh):

time: 30.1 us -> 24.4 us (0.81)
  local copies, waits for them, and re-layouts: 6.46 us -> 1.22 us
  Pallas kernels: 22.8 us -> 22.4 us
    unnamed x4 -> x2, local copies, waits for them, and re-layouts: 6.46 us -> 1.22 us
    pallas_call x1, Pallas kernels: 22.8 us -> 22.4 us  [per_device(): pl.pallas_call(functools.partial(kernel, n_sp, n_tp), out_shape=(jax.Shap...]
where the time goes in v2:
time: 24.4 us; the launch traced here: 24.2 us
  Pallas kernels  22.4 us (92%)
  local copies, waits for them, and re-layouts  1.22 us (5%)
  between operations  0.64 us (3%)
    pallas_call x1, Pallas kernels, per_device(): pl.pallas_call(functools.partial(kernel, n_sp, n_tp), out_shape=(jax.Shap...  22.4 us
    unnamed x2, local copies, waits for them, and re-layouts  1.22 us

profile of v2, /device:TPU:0, one launch (start us, length us, event | category | flops | bytes accessed | tf_op | source)
XLA Modules:
  0.0 24.2 jit_solution(9173222768022123787)
XLA Ops:
  0.6 22.4 %shard_map.158 = (bf16[128,512]{1,0:T(8,128)(2,1)S(1)}, f32[2,128]{1,0:T(2,128)S(1)}) custom-call(bf16[32,2048]{1,0:T(8,128)(2,1)} %tokens_hbm.1, s32[16]{0:T(128)} %lengths_hbm.1, bf16[2048,512]{1,0:T(8,128)(2,1)} %query_down_hbm.1, bf16[2048,256]{1,0:T(8,128)(2,1)} %latent_down_hbm.1, bf16[32,2048]{1,0:T(8,128)(2,1)} %bitcast.8, f32[1,512]{1,0:T(1,128)} %bitcast.9, ...), custom_call_target="tpu_custom_call" | custom-call | tf_op jit(solution)/shard_map/pallas_call | solution.py:396
  23.0 0.7 %copy.19 = bf16[128,512]{1,0:T(8,128)(2,1)} copy(bf16[128,512]{1,0:T(8,128)(2,1)S(1)} %get-tuple-element.4) | data formatting | bytes 262144
  23.7 0.6 %copy.20 = f32[2,128]{1,0:T(2,128)} copy(f32[2,128]{1,0:T(2,128)S(1)} %get-tuple-element.5) | data formatting | bytes 2048

commit v3 on v2

--- a/solution.py
+++ b/solution.py
@@ -68,7 +68,7 @@
     tokens, lengths, query_down, latent_down, rope_down,
     query_latent_gain, latent_gain, query_up, key_up, value_up,
     query_gain, key_gain, output_gain, output_weight, inverse_ref,
-    lat, qlat, heads, load_sem,
+    lat, ropes, qlat, heads, load_sem,
     z_send, z_recv, a_send, a_recv, b_send, b_recv, c_send, c_recv,
     q_send, q_recv, h_send, h_recv,
 ):
@@ -112,16 +112,33 @@
     core = (sp, xor(tp, 1))
 
     def block(device):
-        start = pl.multiple_of((device[0] * n_tp + device[1]) * rows, rows)
-        return lat.at[pl.ds(start, rows)]
+        place = device[0] * n_tp + device[1]
+        return lat.at[pl.ds(pl.multiple_of(place * rows, rows), rows)], ropes.at[place]
+
+    def copies(ref, sends, recvs, index, target):
+        if not isinstance(ref, tuple):
+            ref, index = (ref,), ((index,),)
+        else:
+            index = tuple((part, index) for part in range(len(ref)))
+        return [
+            pltpu.make_async_remote_copy(
+                src_ref=part, dst_ref=part, send_sem=sends.at[place], recv_sem=recvs.at[place],
+                device_id=target, device_id_type=MESH,
+            )
+            for part, place in zip(ref, index)
+        ]
 
     def send(ref, sends, recvs, index, target):
-        copy = pltpu.make_async_remote_copy(
-            src_ref=ref, dst_ref=ref, send_sem=sends.at[index], recv_sem=recvs.at[index],
-            device_id=target, device_id_type=MESH,
-        )
-        copy.start()
-        return copy
+        for copy in copies(ref, sends, recvs, index, target):
+            copy.start()
+
+    def recv(ref, sends, recvs, index, target):
+        for copy in copies(ref, sends, recvs, index, target):
+            copy.wait_recv()
+
+    def sent(ref, sends, recvs, index):
+        for copy in copies(ref, sends, recvs, index, core):
+            copy.wait_send()
 
     def along(device, step):
         return (xor(device[0], 2 * step), device[1])
@@ -130,15 +147,17 @@
     for load in loads[:4]:
         load.wait()
     latent = jnp.dot(tokens[...], latent_down[...], preferred_element_type=F32)
-    rope = nt_dot(tokens[...], rope_down[...])
+    rope = nt_dot(rope_down[...], tokens[...])
     latent = norm_lanes(latent, latent_gain[...]).astype(BF16)
-    rope = jnp.concatenate([rope, jnp.zeros((rows, LANES - ROPE), F32)], axis=1).astype(BF16)
+    rope = jnp.concatenate(
+        [rope[start:start + 8] for start in range(0, ROPE, 8)], axis=1
+    ).astype(BF16)
     own = pl.ds(pl.multiple_of((sp * n_tp + tp) * rows, rows), rows)
-    lat[own, :kvr] = latent
-    lat[own, kvr:] = rope
+    lat[own, :] = latent
+    ropes[sp * n_tp + tp] = rope
     pl.semaphore_wait(barrier, n_outer + n_tp - 1)
 
-    each(n_outer - 1, lambda k: send(block(me), z_send, z_recv, k, along(me, k + 1)) and None)
+    each(n_outer - 1, lambda k: send(block(me), z_send, z_recv, k, along(me, k + 1)))
     send(block(me), a_send, a_recv, 0, first)
     send(block(me), b_send, b_recv, 0, second)
     send(block(me), c_send, c_recv, 0, core)
@@ -178,9 +197,6 @@
     span = min(seq, KEY_CHUNK)
     query_base = sp * group_rows
     query_places = query_base + lax.broadcasted_iota(jnp.int32, (1, group_rows), 1)
-    query_angles = inverse * query_places.astype(F32)
-    query_cos, query_sin = jnp.cos(query_angles), jnp.sin(query_angles)
-    query_docs = docs_of(query_base + lax.broadcasted_iota(jnp.int32, (group_rows, 1), 0))
 
     def key_tables(offset):
         places = offset + lax.broadcasted_iota(jnp.int32, (1, span), 1)
@@ -189,19 +205,6 @@
 
     plain_rows = head_count * NOPE
     key_up_t = jnp.transpose(key_up[...].astype(F32)).astype(BF16)
-    eye = (
-        lax.broadcasted_iota(jnp.int32, (ROPE, LANES), 0)
-        == lax.broadcasted_iota(jnp.int32, (ROPE, LANES), 1)
-    ).astype(F32).astype(BF16)
-    if seq == span:
-        tables = key_tables(0)
-
-    def recv(ref, sends, recvs, index, target):
-        pltpu.make_async_remote_copy(
-            src_ref=ref, dst_ref=ref, send_sem=sends.at[index], recv_sem=recvs.at[index],
-            device_id=target, device_id_type=MESH,
-        ).wait_recv()
-
     def from_first(k):
         source = along(first, k)
         recv(block(source), a_send, a_recv, k, first)
@@ -234,12 +237,12 @@
     send(query_block(xor(tp, 2)), q_send, q_recv, 2, core)
     each(n_outer - 1, lambda k: from_z(k + 1))
     from_both(0)
-
-    def rest(k):
-        from_first(k + 1)
-        from_second(k + 1)
-
-    each(n_outer - 1, rest)
+    each(n_outer - 1, lambda k: from_first(k + 1))
+    query_angles = inverse * query_places.astype(F32)
+    query_cos, query_sin = jnp.cos(query_angles), jnp.sin(query_angles)
+    query_docs = docs_of(query_base + lax.broadcasted_iota(jnp.int32, (group_rows, 1), 0))
+    if seq == span:
+        tables = key_tables(0)
 
     recv(query_block(xor(tp, 1)), q_send, q_recv, 1, core)
     recv(query_block(xor(tp, 3)), q_send, q_recv, 2, core)
@@ -255,6 +258,7 @@
         )
         queries.append(jnp.transpose(piece)[:, :WIDTH].astype(BF16))
 
+    each(n_outer - 1, lambda k: from_second(k + 1))
     each(n_outer - 1, lambda k: from_both(k + 1))
 
     def from_core(k):
@@ -270,12 +274,31 @@
     lane = lax.broadcasted_iota(jnp.int32, (group_rows, out_width), 1)
     score_scale = WIDTH ** (-0.5)
 
+    def unpacked(offset):
+        groups = ROPE // 8
+        lanes = groups * rows
+        segment = lax.broadcasted_iota(jnp.int32, (8, lanes), 1) // rows
+        base = offset // rows
+        columns = []
+        for start in range(0, span // rows, groups):
+            packed = [ropes[base + start + place].astype(F32) for place in range(groups)]
+            bands = []
+            for group in range(groups):
+                band = packed[group]
+                for place in range(groups):
+                    if place != group:
+                        shift = ((place - group) * rows) % lanes
+                        moved = pltpu.roll(packed[place], shift, 1)
+                        band = jnp.where(segment == place, moved, band)
+                bands.append(band)
+            columns.append(jnp.concatenate(bands, axis=0))
+        return jnp.concatenate(columns, axis=1)
+
     def absorb(offset, known, carried):
         cosine, sine, allowed = known
-        block_rows = lat[pl.ds(offset, span), :]
-        latents = block_rows[:, :kvr]
+        latents = lat[pl.ds(offset, span), :]
         plain = nt_dot(key_up_t, latents)
-        shared = nt_dot(eye, block_rows[:, kvr:])
+        shared = unpacked(offset)
         values = jnp.dot(latents, value_up[...], preferred_element_type=F32).astype(BF16)
         shared_square = jnp.sum(shared * shared, axis=0, keepdims=True)
         fresh = []
@@ -344,12 +367,6 @@
     )
     out_ref[...] = jnp.dot(normed, output_weight[...], preferred_element_type=F32).astype(BF16)
 
-    def sent(ref, sends, recvs, index):
-        pltpu.make_async_remote_copy(
-            src_ref=ref, dst_ref=ref, send_sem=sends.at[index], recv_sem=recvs.at[index],
-            device_id=core, device_id_type=MESH,
-        ).wait_send()
-
     each(n_outer - 1, lambda k: sent(block(me), z_send, z_recv, k))
     each(n_outer, lambda k: sent(block(along(me, k)), a_send, a_recv, k))
 
@@ -402,14 +419,15 @@
         in_specs=[pl.BlockSpec(memory_space=pltpu.HBM)] * len(operands),
         out_specs=(pl.BlockSpec(memory_space=pltpu.VMEM),) * 2,
         scratch_shapes=held + [
-            pltpu.VMEM((seq, kvr + LANES), BF16),
+            pltpu.VMEM((seq, kvr), BF16),
+            pltpu.VMEM((seq // rows, 8, ROPE * rows // 8), BF16),
             pltpu.VMEM((group_rows, query_down.shape[1]), BF16),
             pltpu.VMEM((n_tp, group_rows, head_count * VD), BF16),
             dma((len(operands),)),
-            dma((n_outer - 1,)), dma((n_outer - 1,)),
-            dma((n_outer,)), dma((n_outer,)),
-            dma((2 * n_outer,)), dma((2 * n_outer,)),
-            dma((4 * n_outer,)), dma((4 * n_outer,)),
+            dma((2, n_outer - 1)), dma((2, n_outer - 1)),
+            dma((2, n_outer)), dma((2, n_outer)),
+            dma((2, 2 * n_outer)), dma((2, 2 * n_outer)),
+            dma((2, 4 * n_outer)), dma((2, 4 * n_outer)),
             dma((n_tp - 1,)), dma((n_tp - 1,)),
             dma((n_tp - 1,)), dma((n_tp - 1,)),
         ],

time: 24.4 us -> 24.5 us (level)
  no operation moved by 1% of the time
where the time goes in v3:
time: 24.5 us; the launch traced here: 24.4 us
  Pallas kernels  22.5 us (92%)
  local copies, waits for them, and re-layouts  1.22 us (5%)
  between operations  0.64 us (3%)
    pallas_call x1, Pallas kernels, per_device(): pl.pallas_call(functools.partial(kernel, n_sp, n_tp), out_shape=(jax.Shap...  22.5 us
    unnamed x2, local copies, waits for them, and re-layouts  1.22 us

profile of v3, /device:TPU:0, one launch (start us, length us, event | category | flops | bytes accessed | tf_op | source)
XLA Modules:
  0.0 24.4 jit_solution(4136807178160672711)
XLA Ops:
  0.6 22.5 %shard_map.158 = (bf16[128,512]{1,0:T(8,128)(2,1)S(1)}, f32[2,128]{1,0:T(2,128)S(1)}) custom-call(bf16[32,2048]{1,0:T(8,128)(2,1)} %tokens_hbm.1, s32[16]{0:T(128)} %lengths_hbm.1, bf16[2048,512]{1,0:T(8,128)(2,1)} %query_down_hbm.1, bf16[2048,256]{1,0:T(8,128)(2,1)} %latent_down_hbm.1, bf16[32,2048]{1,0:T(8,128)(2,1)} %bitcast.8, f32[1,512]{1,0:T(1,128)} %bitcast.9, ...), custom_call_target="tpu_custom_call" | custom-call | tf_op jit(solution)/shard_map/pallas_call | solution.py:413
  23.2 0.7 %copy.19 = bf16[128,512]{1,0:T(8,128)(2,1)} copy(bf16[128,512]{1,0:T(8,128)(2,1)S(1)} %get-tuple-element.4) | data formatting | bytes 262144
  23.8 0.6 %copy.20 = f32[2,128]{1,0:T(2,128)} copy(f32[2,128]{1,0:T(2,128)S(1)} %get-tuple-element.5) | data formatting | bytes 2048

commit v4 on v3

--- a/solution.py
+++ b/solution.py
@@ -103,6 +103,9 @@
 
     each(n_outer - 1, greet)
     pl.semaphore_signal(barrier, inc=1, device_id=(xor(sp, 1), tp), device_id_type=MESH)
+    pl.semaphore_signal(
+        barrier, inc=1, device_id=(xor(sp, 1), xor(tp, 2)), device_id_type=MESH
+    )
     for other in range(1, n_tp):
         pl.semaphore_signal(barrier, inc=1, device_id=(sp, xor(tp, other)), device_id_type=MESH)
 
@@ -110,6 +113,7 @@
     first = (xor(sp, 1 - parity), xor(tp, 2 * parity))
     second = (xor(sp, parity), xor(tp, 2 * (1 - parity)))
     core = (sp, xor(tp, 1))
+    corner = (xor(sp, 1), xor(tp, 2))
 
     def block(device):
         place = device[0] * n_tp + device[1]
@@ -155,11 +159,12 @@
     own = pl.ds(pl.multiple_of((sp * n_tp + tp) * rows, rows), rows)
     lat[own, :] = latent
     ropes[sp * n_tp + tp] = rope
-    pl.semaphore_wait(barrier, n_outer + n_tp - 1)
+    pl.semaphore_wait(barrier, n_outer + n_tp)
 
     each(n_outer - 1, lambda k: send(block(me), z_send, z_recv, k, along(me, k + 1)))
     send(block(me), a_send, a_recv, 0, first)
     send(block(me), b_send, b_recv, 0, second)
+    send(block(me), b_send, b_recv, 1, corner)
     send(block(me), c_send, c_recv, 0, core)
 
     for load in loads[4:6]:
@@ -208,7 +213,6 @@
     def from_first(k):
         source = along(first, k)
         recv(block(source), a_send, a_recv, k, first)
-        send(block(source), b_send, b_recv, 2 * k + 1, second)
         send(block(source), c_send, c_recv, 4 * k + 1, core)
 
     def from_z(k):
@@ -216,6 +220,7 @@
         recv(block(source), z_send, z_recv, k - 1, source)
         send(block(source), a_send, a_recv, k, first)
         send(block(source), b_send, b_recv, 2 * k, second)
+        send(block(source), b_send, b_recv, 2 * k + 1, corner)
         send(block(source), c_send, c_recv, 4 * k, core)
 
     def both(k):
@@ -228,7 +233,7 @@
 
     def from_both(k):
         source = both(k)
-        recv(block(source), b_send, b_recv, 2 * k + 1, second)
+        recv(block(source), b_send, b_recv, 2 * k + 1, corner)
         send(block(source), c_send, c_recv, 4 * k + 3, core)
 
     from_first(0)
@@ -372,7 +377,7 @@
 
     def sent_rest(k):
         sent(block(along(me, k)), b_send, b_recv, 2 * k)
-        sent(block(along(first, k)), b_send, b_recv, 2 * k + 1)
+        sent(block(along(me, k)), b_send, b_recv, 2 * k + 1)
         sent(block(along(me, k)), c_send, c_recv, 4 * k)
         sent(block(along(first, k)), c_send, c_recv, 4 * k + 1)
         sent(block(along(second, k)), c_send, c_recv, 4 * k + 2)

time: 24.5 us -> 22.8 us (0.931)
  Pallas kernels: 22.5 us -> 20.8 us
    pallas_call x1, Pallas kernels: 22.5 us -> 20.8 us  [per_device(): pl.pallas_call(functools.partial(kernel, n_sp, n_tp), out_shape=(jax.Shap...]
where the time goes in v4:
time: 22.8 us; the launch traced here: 22.7 us
  Pallas kernels  20.8 us (91%)
  local copies, waits for them, and re-layouts  1.22 us (5%)
  between operations  0.64 us (3%)
    pallas_call x1, Pallas kernels, per_device(): pl.pallas_call(functools.partial(kernel, n_sp, n_tp), out_shape=(jax.Shap...  20.8 us
    unnamed x2, local copies, waits for them, and re-layouts  1.22 us

profile of v4, /device:TPU:0, one launch (start us, length us, event | category | flops | bytes accessed | tf_op | source)
XLA Modules:
  0.0 22.7 jit_solution(5423477335822632161)
XLA Ops:
  0.6 20.8 %shard_map.158 = (bf16[128,512]{1,0:T(8,128)(2,1)S(1)}, f32[2,128]{1,0:T(2,128)S(1)}) custom-call(bf16[32,2048]{1,0:T(8,128)(2,1)} %tokens_hbm.1, s32[16]{0:T(128)} %lengths_hbm.1, bf16[2048,512]{1,0:T(8,128)(2,1)} %query_down_hbm.1, bf16[2048,256]{1,0:T(8,128)(2,1)} %latent_down_hbm.1, bf16[32,2048]{1,0:T(8,128)(2,1)} %bitcast.8, f32[1,512]{1,0:T(1,128)} %bitcast.9, ...), custom_call_target="tpu_custom_call" | custom-call | tf_op jit(solution)/shard_map/pallas_call | solution.py:418
  21.5 0.7 %copy.19 = bf16[128,512]{1,0:T(8,128)(2,1)} copy(bf16[128,512]{1,0:T(8,128)(2,1)S(1)} %get-tuple-element.4) | data formatting | bytes 262144
  22.1 0.6 %copy.20 = f32[2,128]{1,0:T(2,128)} copy(f32[2,128]{1,0:T(2,128)S(1)} %get-tuple-element.5) | data formatting | bytes 2048
